TPU v7x, 32 devices: a whole 2x2x4 slice. The times are simulated.
32 devices in a mesh: sp: 8 (over z, x), dp: 4 (over y, core).
Axes of the slice: x: 2, y: 2, z: 4, core: 2. Of those that a mesh axis runs over, the one named last changes fastest.
Arguments:
- inputs: bfloat16 [1536, 2048], P('sp'), may hold values from -6 to 6
- w_query: bfloat16 [2048, 2048], P('dp'), may hold values from -0.125 to 0.125
- w_key: bfloat16 [1024, 2048], P('dp'), may hold values from -0.125 to 0.125
- w_value: bfloat16 [1024, 2048], P('dp'), may hold values from -0.125 to 0.125
- query_gain: float32 [64], replicated, may hold values from 0.6 to 7
- key_gain: float32 [64], replicated, may hold values from 0.6 to 7
- grad_out: bfloat16 [1536, 2048], P('sp', 'dp'), may hold values from -6 to 6
Outputs:
- d_inputs: bfloat16 [1536, 2048], P('sp', 'dp')
- grad_wq: float32 [2048, 2048], P('dp')
- grad_wk: float32 [1024, 2048], P('dp')
- grad_wv: float32 [1024, 2048], P('dp')
All inputs are finite; a program needn't handle non-finite values.
Results may differ from a plain program's by a relative error of at most 0.019.
The roundings to bfloat16 on the way count: a program that leaves them out, or rounds other values in their place, can miss the bound.
Values may be sent and summed in bfloat16 or wider, within the bound.
A program may use at most 64 MiB of HBM per device.

v0:
```python
import jax
import jax.numpy as jnp
from jax import lax
from jax.sharding import PartitionSpec as P

HEAD_WIDTH = 64
GRID_W = 64


norm_eps = 1e-06
axial_base = 10000.0


def rotation_tables(offset, count):
    positions = offset + jnp.arange(count, dtype=jnp.int32)
    grid_rows = (positions // GRID_W).astype(jnp.float32)
    grid_cols = (positions % GRID_W).astype(jnp.float32)
    quarter = HEAD_WIDTH // 4
    freqs_axis = axial_base ** (-jnp.arange(quarter, dtype=jnp.float32) / quarter)
    angle_rows = grid_rows[:, None] * freqs_axis[None, :]
    angle_cols = grid_cols[:, None] * freqs_axis[None, :]
    cosine = jnp.concatenate(
        [jnp.cos(angle_rows), jnp.cos(angle_rows), jnp.cos(angle_cols), jnp.cos(angle_cols)], axis=1
    )
    sine = jnp.concatenate(
        [jnp.sin(angle_rows), jnp.sin(angle_rows), jnp.sin(angle_cols), jnp.sin(angle_cols)], axis=1
    )
    return (cosine, sine)


def quarter_turn(values):
    quarter = HEAD_WIDTH // 4
    return jnp.concatenate(
        [
            -values[..., quarter : 2 * quarter],
            values[..., :quarter],
            -values[..., 3 * quarter :],
            values[..., 2 * quarter : 3 * quarter],
        ],
        axis=-1,
    )


def quarter_back(values):
    quarter = HEAD_WIDTH // 4
    return jnp.concatenate(
        [
            values[..., quarter : 2 * quarter],
            -values[..., :quarter],
            values[..., 3 * quarter :],
            -values[..., 2 * quarter : 3 * quarter],
        ],
        axis=-1,
    )


def rotate(values, cosine, sine):
    return values * cosine + quarter_turn(values) * sine


def rotate_back(grads, cosine, sine):
    return grads * cosine + quarter_back(grads * sine)


def head_norm(raw):
    scale_inv = lax.rsqrt(jnp.mean(raw * raw, axis=-1, keepdims=True) + norm_eps)
    return (raw * scale_inv, scale_inv)


def head_norm_back(grads, normed, scale_inv, gain):
    scaled = grads * gain
    return scale_inv * (scaled - normed * jnp.mean(scaled * normed, axis=-1, keepdims=True))


def body(inputs, w_query, w_key, w_value, query_gain, key_gain, grad_out):
    tok_rows = inputs.shape[0]
    local_query = w_query.shape[0] // HEAD_WIDTH
    local_keys = w_key.shape[0] // HEAD_WIDTH
    group = local_query // local_keys
    key_width = local_keys * HEAD_WIDTH
    scale = HEAD_WIDTH ** (-0.5)
    contract = (((1,), (1,)), ((), ()))
    leading = (((0,), (0,)), ((), ()))
    offset = lax.axis_index("sp") * tok_rows
    cosine, sine = rotation_tables(offset, tok_rows)
    cos_wide = cosine[:, None, :]
    sin_wide = sine[:, None, :]
    q_raw = lax.dot_general(inputs, w_query, contract, preferred_element_type=jnp.float32).astype(
        jnp.bfloat16
    )
    w_pair = jnp.concatenate([w_key, w_value], axis=0)
    kv_raw = lax.dot_general(inputs, w_pair, contract, preferred_element_type=jnp.float32).astype(
        jnp.bfloat16
    )
    q_wide = (
        lax.optimization_barrier(q_raw)
        .astype(jnp.float32)
        .reshape(tok_rows, local_query, HEAD_WIDTH)
    )
    k_wide = (
        lax.optimization_barrier(kv_raw[:, :key_width])
        .astype(jnp.float32)
        .reshape(tok_rows, local_keys, HEAD_WIDTH)
    )
    q_normed, q_inv = head_norm(q_wide)
    k_normed, k_inv = head_norm(k_wide)
    q_rot = rotate(q_normed * query_gain, cos_wide, sin_wide).astype(jnp.bfloat16)
    k_rot = rotate(k_normed * key_gain, cos_wide, sin_wide).astype(jnp.bfloat16)
    kv_rot = jnp.concatenate([k_rot.reshape(tok_rows, key_width), kv_raw[:, key_width:]], axis=1)
    kv_every = lax.all_gather(kv_rot, "sp", axis=0, tiled=True)
    seq_rows = kv_every.shape[0]
    keys_every = kv_every[:, :key_width]
    values_every = kv_every[:, key_width:]
    grad_query = []
    log_totals = []
    deltas = []
    key_terms = [jnp.zeros((seq_rows, HEAD_WIDTH), jnp.float32) for slot in range(local_keys)]
    value_terms = [jnp.zeros((seq_rows, HEAD_WIDTH), jnp.float32) for slot in range(local_keys)]
    for member in range(local_query):
        kv_index = member // group
        query_head = q_rot[:, member, :]
        key_head = keys_every[:, kv_index * HEAD_WIDTH : (kv_index + 1) * HEAD_WIDTH]
        value_head = values_every[:, kv_index * HEAD_WIDTH : (kv_index + 1) * HEAD_WIDTH]
        grad_head = grad_out[:, member * HEAD_WIDTH : (member + 1) * HEAD_WIDTH]
        scores = (
            lax.dot_general(query_head, key_head, contract, preferred_element_type=jnp.float32)
            * scale
        )
        maxima = jnp.max(scores, axis=1, keepdims=True)
        log_total = maxima + jnp.log(jnp.sum(jnp.exp(scores - maxima), axis=1, keepdims=True))
        prob_exact = jnp.exp(scores - log_total)
        prob_half = prob_exact.astype(jnp.bfloat16)
        attn_rows = jnp.dot(prob_half, value_head, preferred_element_type=jnp.float32).astype(
            jnp.bfloat16
        )
        attn_wide = lax.optimization_barrier(attn_rows).astype(jnp.float32)
        delta_rows = jnp.sum(grad_head.astype(jnp.float32) * attn_wide, axis=1, keepdims=True)
        dprob = lax.dot_general(grad_head, value_head, contract, preferred_element_type=jnp.float32)
        dscore = (prob_exact * (dprob - delta_rows)).astype(jnp.bfloat16)
        grad_query.append(jnp.dot(dscore, key_head, preferred_element_type=jnp.float32) * scale)
        log_totals.append(log_total)
        deltas.append(delta_rows)
        value_terms[kv_index] = value_terms[kv_index] + lax.dot_general(
            prob_half, grad_head, leading, preferred_element_type=jnp.float32
        )
        key_terms[kv_index] = (
            key_terms[kv_index]
            + lax.dot_general(dscore, query_head, leading, preferred_element_type=jnp.float32)
            * scale
        )
    gradient_query_rotated = jnp.stack(grad_query, axis=1)
    partial_sums = jnp.concatenate(key_terms + value_terms, axis=1)
    own_grads = lax.psum_scatter(partial_sums, "sp", scatter_dimension=0, tiled=True)
    gradient_key_rotated = own_grads[:, :key_width].reshape(tok_rows, local_keys, HEAD_WIDTH)
    grad_q = head_norm_back(
        rotate_back(gradient_query_rotated, cos_wide, sin_wide), q_normed, q_inv, query_gain
    )
    grad_q = grad_q.reshape(tok_rows, local_query * HEAD_WIDTH).astype(jnp.bfloat16)
    grad_k = head_norm_back(
        rotate_back(gradient_key_rotated, cos_wide, sin_wide), k_normed, k_inv, key_gain
    )
    grad_kv = jnp.concatenate(
        [
            grad_k.reshape(tok_rows, key_width).astype(jnp.bfloat16),
            own_grads[:, key_width:].astype(jnp.bfloat16),
        ],
        axis=1,
    )
    head_part = jnp.dot(grad_q, w_query, preferred_element_type=jnp.float32)
    head_part = head_part + jnp.dot(grad_kv, w_pair, preferred_element_type=jnp.float32)
    d_inputs = lax.psum_scatter(
        head_part.astype(jnp.bfloat16), "dp", scatter_dimension=1, tiled=True
    )
    grad_wq = lax.dot_general(grad_q, inputs, leading, preferred_element_type=jnp.float32)
    grad_wkv = lax.dot_general(grad_kv, inputs, leading, preferred_element_type=jnp.float32)
    grad_wq, grad_wkv = lax.psum((grad_wq, grad_wkv), "sp")
    return (d_inputs, grad_wq, grad_wkv[:key_width], grad_wkv[key_width:])


def solution(mesh):
    return jax.shard_map(
        body,
        mesh=mesh,
        in_specs=(
            P("sp", None),
            P("dp", None),
            P("dp", None),
            P("dp", None),
            P(),
            P(),
            P("sp", "dp"),
        ),
        out_specs=(P("sp", "dp"), P("dp", None), P("dp", None), P("dp", None)),
        check_vma=False,
    )
```

profile of v0, /device:TPU:0, one launch (start us, length us, event | category | flops | bytes accessed | tf_op | source)
XLA Modules:
  0.0 498.9 jit_solution(4581374337283304342)
XLA Ops:
  7.3 0.8 mul.353
  8.1 0.8 multiply_cosine_fusion.1
  9.1 1.4 constant_dynamic-update-slice_fusion.1
  10.8 1.0 copy-done.3
  11.9 0.8 fusion.37
  13.9 1.0 copy.94
  15.1 0.8 pad_maximum_fusion.6
  15.9 0.7 maximum_multiply_fusion.1
  16.6 1.7 copy.97
  18.3 0.7 mul.350
  19.1 1.1 copy.95
  20.2 1.1 add_convert_fusion
  21.3 1.6 pad_maximum_fusion.1
  22.9 1.5 convolution_convert_fusion.1
  24.5 0.7 fusion.145
  25.2 1.5 copy.126
  26.7 1.5 copy.125
  28.9 0.7 copy.123
  30.3 0.7 copy.121
  31.0 0.7 copy.120
  31.7 0.7 copy.119
  32.4 1.1 copy.93
  33.7 0.9 fusion.63
  34.6 35.3 %all-gather.2.cloned.1.call-done = bf16[1536,512]{1,0:T(8,128)(2,1)} async-done(((bf16[192,512]{1,0:T(8,128)(2,1)}), bf16[1536,512]{1,0:T(8,128)(2,1)}) %all-gather.2.cloned.1.call-update) | async-done | bytes 1572880 | tf_op jit(solution)/shard_map/all_gather | solution.py:110
  69.9 1.6 fusion.148
  88.3 0.9 copy-done.18
  89.1 1.0 fusion.36
  90.5 0.8 copy-done.16
  91.3 1.0 fusion.34
  92.7 0.8 copy-done.14
  93.5 1.0 fusion.32
  94.9 1.0 fusion.30
  95.9 1.1 fusion.28
  97.1 1.1 fusion.27
  98.2 1.1 fusion.26
  99.3 1.1 fusion.25
  100.5 3.5 copy.117
  105.4 0.8 mul.334
  106.2 2.0 copy.109
  108.3 1.6 fusion.53
  109.9 1.6 fusion.51
  111.5 1.7 fusion.49
  116.6 1.6 multiply_reduce_fusion
  118.2 2.0 copy.106
  120.9 0.9 copy.108
  121.8 1.4 multiply_convert_fusion
  123.2 2.8 fusion.156
  126.0 51.0 %reduce-scatter.7.cloned.1.call-done = f32[192,512]{1,0:T(8,128)} async-done(((f32[1536,512]{1,0:T(8,128)}), f32[192,512]{1,0:T(8,128)}) %reduce-scatter.7.cloned.1.call-update) | async-done | bytes 393232 | tf_op jit(solution)/shard_map/reduce_scatter | solution.py:153
  177.0 1.6 slice.233
  178.6 1.8 copy.112
  180.4 1.0 broadcast_multiply_fusion.1
  181.5 1.6 pad_maximum_fusion
  183.1 1.8 copy.113
  184.9 0.7 mul.421
  185.7 1.7 copy.114
  187.4 0.9 slice.371
  188.4 1.3 multiply_convert_fusion.1
  190.3 2.7 fusion.96
  194.0 0.8 copy-done.20
  194.8 1.5 fusion.16
  196.3 266.0 %all-reduce.3.cloned.1.call-done = (f32[512,2048]{1,0:T(8,128)}, f32[512,2048]{1,0:T(8,128)}) async-done(((f32[512,2048]{1,0:T(8,128)}, f32[512,2048]{1,0:T(8,128)}), (f32[512,2048]{1,0:T(8,128)}, f32[512,2048]{1,0:T(8,128)})) %all-reduce.3.cloned.1.call-update) | async-done | bytes 8388624 | tf_op jit(solution)/shard_map/psum | solution.py:176
  462.3 4.7 fusion.142
  467.0 20.6 %reduce-scatter.5.cloned.1.call-done = bf16[192,512]{1,0:T(8,128)(2,1)} async-done(((bf16[192,2048]{1,0:T(8,128)(2,1)}), bf16[192,512]{1,0:T(8,128)(2,1)}) %reduce-scatter.5.cloned.1.call-update) | async-done | bytes 196624 | tf_op jit(solution)/shard_map/reduce_scatter | solution.py:171
  487.7 4.7 copy.144
  (190 shorter events, 28.4 us)
Async XLA Ops:
  7.2 15.8 %copy-start = (bf16[512,2048]{1,0:T(8,128)(2,1)S(1)}, bf16[512,2048]{1,0:T(8,128)(2,1)}, u32[]{:S(2)}) copy-start(bf16[512,2048]{1,0:T(8,128)(2,1)} %param.8) | copy-start | bytes 6291460
  7.2 62.7 %all-gather.2.cloned.1.call-start = ((), (), s32[]{:S(2)}) async-start(), calls=%async_computation.2 | async-start | bytes 1769472 | tf_op jit(solution)/shard_map/all_gather | solution.py:110
  8.1 12.0 %copy-start.43 = (f32[256]{0:T(256)}, f32[256]{0:T(256)S(1)}, u32[]{:S(2)}) copy-start(f32[256]{0:T(256)S(1)} %mul.354) | copy-start | bytes 3076
  9.0 107.1 %copy-start.29 = (f32[192,64]{0,1:T(8,128)}, f32[192,64]{0,1:T(8,128)S(1)}, u32[]{:S(2)}) copy-start(f32[192,64]{0,1:T(8,128)S(1)} %pad_maximum_fusion.5) | copy-start | bytes 147460
  9.1 11.0 %copy-start.25 = (f32[192,256]{1,0:T(8,128)}, f32[192,256]{1,0:T(8,128)S(1)}, u32[]{:S(2)}) copy-start(f32[192,256]{1,0:T(8,128)S(1)} %copy.96) | copy-start | bytes 589828
  9.1 1.6 copy-start.30
  10.7 1.1 copy-start.3
  11.9 1.3 copy-start.19
  11.9 3.1 copy-start.48
  14.9 3.5 copy-start.21
  20.1 2.7 copy-start.27
  22.9 1.6 copy-start.4
  22.9 154.1 %reduce-scatter.7.cloned.1.call-start = ((), (), s32[]{:S(2)}) async-start(), calls=%async_computation.4 | async-start | bytes 3538944 | tf_op jit(solution)/shard_map/reduce_scatter | solution.py:153
  24.5 9.1 %copy-start.45 = (f32[64]{0:T(128)S(1)}, f32[64]{0:T(128)}, u32[]{:S(2)}) copy-start(f32[64]{0:T(128)} %param.11) | copy-start | bytes 772
  69.9 1.9 copy-start.1
  71.5 1.0 copy-start.23
  76.5 0.9 copy-start.5
  77.8 0.8 copy-start.42
  79.1 0.8 copy-start.6
  80.6 0.8 copy-start.41
  81.8 0.8 copy-start.8
  83.3 0.8 copy-start.40
  84.5 0.8 copy-start.10
  86.1 0.8 copy-start.39
  86.9 0.8 copy-start.38
  86.9 0.8 copy-start.37
  86.9 0.9 copy-start.36
  86.9 0.9 copy-start.35
  87.3 1.0 copy-start.11
  88.2 0.9 copy-start.18
  90.5 0.8 copy-start.16
  92.7 0.8 copy-start.14
  94.9 2.1 copy-start.12
  104.0 358.3 %all-reduce.3.cloned.1.call-start = ((), (), s32[]{:S(2)}) async-start(), calls=%async_computation.5 | async-start | bytes 16777216 | tf_op jit(solution)/shard_map/psum | solution.py:176
  108.3 3.2 copy-start.2
  109.9 3.3 copy-start.17
  111.5 2.2 copy-start.9
  113.2 1.1 copy-start.15
  113.7 1.1 copy-start.7
  114.2 1.1 copy-start.13
  115.9 0.7 copy-start.46
  118.1 3.7 copy-start.47
  126.0 55.5 %copy-start.22 = (f32[192,256]{0,1:T(8,128)S(1)}, f32[192,256]{0,1:T(8,128)}, u32[]{:S(2)}) copy-start(f32[192,256]{0,1:T(8,128)} %copy-done.21) | copy-start | bytes 589828
  126.0 55.5 %copy-start.49 = (f32[64]{0:T(128)S(1)}, f32[64]{0:T(128)}, u32[]{:S(2)}) copy-start(f32[64]{0:T(128)} %param.12) | copy-start | bytes 772
  180.4 1.1 copy-start.24
  181.5 6.8 %copy-start.26 = (f32[192,256]{1,0:T(8,128)S(1)}, f32[192,256]{1,0:T(8,128)}, u32[]{:S(2)}) copy-start(f32[192,256]{1,0:T(8,128)} %copy-done.25) | copy-start | bytes 589828
  181.5 6.8 %copy-start.44 = (f32[256]{0:T(256)S(1)}, f32[256]{0:T(256)}, u32[]{:S(2)}) copy-start(f32[256]{0:T(256)} %copy-done.43) | copy-start | bytes 3076
  183.1 5.2 %copy-start.28 = (f32[192,256]{1,0:T(8,128)S(1)}, f32[192,256]{1,0:T(8,128)}, u32[]{:S(2)}) copy-start(f32[192,256]{1,0:T(8,128)} %copy-done.27) | copy-start | bytes 589828
  188.4 1.3 copy-start.31
  189.7 0.6 copy-start.33
  193.1 0.9 copy-start.32
  193.1 0.9 copy-start.34
  193.1 294.6 %reduce-scatter.5.cloned.1.call-start = ((), (), s32[]{:S(2)}) async-start(), calls=%async_computation.3 | async-start | bytes 983040 | tf_op jit(solution)/shard_map/reduce_scatter | solution.py:171
  193.1 1.6 copy-start.20
Sparse Core Ops, SparseCore 0:
  23.0 46.8 all-gather.1
  104.2 72.8 reduce-scatter.6
  193.2 269.0 all-reduce.2
  465.3 22.3 reduce-scatter.4
where the time goes:
time: 500 us; the launch traced here: 499 us
  waiting for transfers between devices  373 us (75%)
  local copies, waits for them, and re-layouts  54.1 us (11%)
  matrix products  40.2 us (8%)
  other arithmetic  16.9 us (3%)
  between operations  14.6 us (3%)
    psum x1, waiting for transfers between devices, body(): grad_wq, grad_wkv = lax.psum((grad_wq, grad_wkv), 'sp')  266 us
    reduce_scatter x1, waiting for transfers between devices, body(): lax.psum_scatter(partial_sums, 'sp', scatter_dimension=0, tiled=True)  51 us
    all_gather x1, waiting for transfers between devices, body(): kv_every = lax.all_gather(kv_rot, 'sp', axis=0, tiled=True)  35.3 us
    unnamed x112, local copies, waits for them, and re-layouts  26.3 us
    reduce_scatter x1, waiting for transfers between devices, body(): lax.psum_scatter(head_part.astype(jnp.bfloat16), 'dp', scatter_dimension=...  20.6 us
  transfers between devices with their start and end apart: 4, of which 4 were waited for; matrix products, arithmetic and copies ran while one was open for 8% of the time, Pallas kernels for 0%

commit v1 on v0

--- a/solution.py
+++ b/solution.py
@@ -1,6 +1,10 @@
+import functools
+
 import jax
 import jax.numpy as jnp
 from jax import lax
+from jax.experimental import pallas as pl
+from jax.experimental.pallas import tpu as pltpu
 from jax.sharding import PartitionSpec as P
 
 HEAD_WIDTH = 64
@@ -177,9 +181,446 @@
     return (d_inputs, grad_wq, grad_wkv[:key_width], grad_wkv[key_width:])
 
 
+MESH = pl.DeviceIdType.MESH
+VMEM_LIMIT = 60 * 1024 * 1024
+
+
+def turn(values):
+    quarter = HEAD_WIDTH // 4
+    return jnp.concatenate(
+        [
+            -values[quarter : 2 * quarter],
+            values[:quarter],
+            -values[3 * quarter :],
+            values[2 * quarter : 3 * quarter],
+        ],
+        axis=0,
+    )
+
+
+def turn_back(values):
+    return -turn(values)
+
+
+def norm_cols(raw):
+    inv = lax.rsqrt(jnp.mean(raw * raw, axis=0, keepdims=True) + norm_eps)
+    return raw * inv, inv
+
+
+def norm_cols_back(grads, normed, inv, gain):
+    scaled = grads * gain
+    return inv * (scaled - normed * jnp.mean(scaled * normed, axis=0, keepdims=True))
+
+
+def other_of_pair(index):
+    return index + 1 - 2 * lax.rem(index, 2)
+
+
+def gather_kernel(n, x_ref, g_ref, xall, gall, xsend, xrecv, gsend, grecv, fsend, frecv, own):
+    me = lax.axis_index("sp")
+    core = lax.rem(lax.axis_index("dp"), 2)
+    twin = other_of_pair(lax.axis_index("dp"))
+    half = x_ref.shape[0] // 2
+    mine = pl.ds(pl.multiple_of(core * half, 16), half)
+    theirs = pl.ds(pl.multiple_of((1 - core) * half, 16), half)
+    barrier = pltpu.get_barrier_semaphore()
+    for off in range(1, n):
+        pl.semaphore_signal(
+            barrier, inc=1, device_id={"sp": lax.rem(me + off, n)}, device_id_type=MESH
+        )
+    pl.semaphore_signal(barrier, inc=1, device_id={"dp": twin}, device_id_type=MESH)
+    pl.semaphore_wait(barrier, n)
+    sends = []
+    for off in range(1, n):
+        peer = lax.rem(me + off, n)
+        sends.append(
+            pltpu.make_async_remote_copy(
+                src_ref=g_ref.at[peer],
+                dst_ref=gall.at[me],
+                send_sem=gsend.at[off - 1],
+                recv_sem=grecv.at[off - 1],
+                device_id={"sp": peer},
+                device_id_type=MESH,
+            )
+        )
+        sends.append(
+            pltpu.make_async_remote_copy(
+                src_ref=x_ref.at[mine],
+                dst_ref=xall.at[me, mine],
+                send_sem=xsend.at[off - 1],
+                recv_sem=xrecv.at[off - 1],
+                device_id={"sp": peer},
+                device_id_type=MESH,
+            )
+        )
+    for copy in sends:
+        copy.start()
+    own_x = pltpu.make_async_copy(x_ref, xall.at[me], own.at[0])
+    own_g = pltpu.make_async_copy(g_ref.at[me], gall.at[me], own.at[1])
+    own_x.start()
+    own_g.start()
+    for off in range(1, n):
+        source = lax.rem(me + n - off, n)
+        pltpu.make_async_remote_copy(
+            src_ref=xall.at[source, mine],
+            dst_ref=xall.at[source, mine],
+            send_sem=xsend.at[off - 1],
+            recv_sem=xrecv.at[off - 1],
+            device_id={"sp": source},
+            device_id_type=MESH,
+        ).wait_recv()
+        pltpu.make_async_remote_copy(
+            src_ref=xall.at[source, mine],
+            dst_ref=xall.at[source, mine],
+            send_sem=fsend.at[off - 1],
+            recv_sem=frecv.at[off - 1],
+            device_id={"dp": twin},
+            device_id_type=MESH,
+        ).start()
+    for off in range(1, n):
+        source = lax.rem(me + n - off, n)
+        pltpu.make_async_remote_copy(
+            src_ref=g_ref.at[source],
+            dst_ref=gall.at[source],
+            send_sem=gsend.at[off - 1],
+            recv_sem=grecv.at[off - 1],
+            device_id={"sp": source},
+            device_id_type=MESH,
+        ).wait_recv()
+        forward = pltpu.make_async_remote_copy(
+            src_ref=xall.at[source, mine],
+            dst_ref=xall.at[source, theirs],
+            send_sem=fsend.at[off - 1],
+            recv_sem=frecv.at[off - 1],
+            device_id={"dp": twin},
+            device_id_type=MESH,
+        )
+        forward.wait()
+    for copy in sends:
+        copy.wait_send()
+    own_x.wait()
+    own_g.wait()
+
+
+def gather_call(n, x, g_parts):
+    rows, width = x.shape
+    dma = pltpu.SemaphoreType.DMA
+    return pl.pallas_call(
+        functools.partial(gather_kernel, n),
+        out_shape=(
+            jax.ShapeDtypeStruct((n, rows, width), x.dtype),
+            jax.ShapeDtypeStruct(g_parts.shape, g_parts.dtype),
+        ),
+        in_specs=[pl.BlockSpec(memory_space=pltpu.VMEM)] * 2,
+        out_specs=[pl.BlockSpec(memory_space=pl.ANY)] * 2,
+        scratch_shapes=[dma((n - 1,))] * 6 + [dma((2,))],
+        compiler_params=pltpu.CompilerParams(
+            collective_id=0, has_side_effects=True, vmem_limit_bytes=VMEM_LIMIT
+        ),
+        name="gather_tokens",
+    )(x, g_parts)
+
+
+def head_kernel(
+    tile, x_ref, w_ref, g_ref, cos_ref, sin_ref, qg_ref, kg_ref,
+    gq_ref, mine_ref, theirs_ref, kn_ref, rk_ref,
+    q_t, q_n, q_r, k_t, v_t, k_s, v_s, g_t, k_n, k_r, dk, dv,
+):
+    seq = x_ref.shape[0]
+    width = HEAD_WIDTH
+    scale = width ** (-0.5)
+    contract = (((1,), (1,)), ((), ()))
+
+    @pl.loop(0, seq // tile)
+    def _(step):
+        cols = pl.ds(pl.multiple_of(step * tile, tile), tile)
+        raw = lax.dot_general(
+            w_ref[...], x_ref[cols, :], contract, preferred_element_type=jnp.float32
+        ).astype(jnp.bfloat16)
+        wide = raw.astype(jnp.float32)
+        cosine = cos_ref[:, cols]
+        sine = sin_ref[:, cols]
+        normed, inv = norm_cols(wide[:width])
+        gained = normed * qg_ref[...]
+        rot = (gained * cosine + turn(gained) * sine).astype(jnp.bfloat16)
+        q_t[:, cols] = (rot.astype(jnp.float32) * scale).astype(jnp.bfloat16)
+        q_n[:, cols] = normed
+        q_r[:, cols] = inv
+        normed, inv = norm_cols(wide[width : 2 * width])
+        gained = normed * kg_ref[...]
+        rot = (gained * cosine + turn(gained) * sine).astype(jnp.bfloat16)
+        k_t[:, cols] = rot
+        k_s[cols, :] = rot.astype(jnp.float32).T.astype(jnp.bfloat16)
+        k_n[:, cols] = normed
+        k_r[:, cols] = inv
+        v_t[:, cols] = raw[2 * width :]
+        v_s[cols, :] = wide[2 * width :].T.astype(jnp.bfloat16)
+        g_t[:, cols] = g_ref[cols, :].astype(jnp.float32).T.astype(jnp.bfloat16)
+
+    dk[...] = jnp.zeros_like(dk)
+    dv[...] = jnp.zeros_like(dv)
+
+    @pl.loop(0, seq // tile)
+    def _(step):
+        cols = pl.ds(pl.multiple_of(step * tile, tile), tile)
+        query = q_t[:, cols]
+        grad = g_t[:, cols]
+        scores = jnp.dot(k_s[...], query, preferred_element_type=jnp.float32)
+        maxima = jnp.max(scores, axis=0, keepdims=True)
+        powers = jnp.exp(scores - maxima)
+        prob = powers * (1.0 / jnp.sum(powers, axis=0, keepdims=True))
+        prob_half = prob.astype(jnp.bfloat16)
+        attn = jnp.dot(v_t[...], prob_half, preferred_element_type=jnp.float32).astype(jnp.bfloat16)
+        delta = jnp.sum(grad.astype(jnp.float32) * attn.astype(jnp.float32), axis=0, keepdims=True)
+        dv[...] += lax.dot_general(grad, prob_half, contract, preferred_element_type=jnp.float32)
+        dprob = jnp.dot(v_s[...], grad, preferred_element_type=jnp.float32)
+        dscore = (prob * (dprob - delta)).astype(jnp.bfloat16)
+        dk[...] += lax.dot_general(query, dscore, contract, preferred_element_type=jnp.float32)
+        dq = jnp.dot(k_t[...], dscore, preferred_element_type=jnp.float32) * scale
+        back = dq * cos_ref[:, cols] + turn_back(dq * sin_ref[:, cols])
+        gq_ref[:, cols] = norm_cols_back(back, q_n[:, cols], q_r[:, cols], qg_ref[...]).astype(
+            jnp.bfloat16
+        )
+
+    parity = lax.rem(lax.axis_index("sp"), 2)
+    half = seq // 2
+    own = pl.ds(pl.multiple_of(parity * half, 128), half)
+    other = pl.ds(pl.multiple_of((1 - parity) * half, 128), half)
+    mine_ref[0] = dk[:, own]
+    mine_ref[1] = dv[:, own]
+    theirs_ref[0] = dk[:, other].astype(jnp.bfloat16)
+    theirs_ref[1] = dv[:, other].astype(jnp.bfloat16)
+    kn_ref[...] = k_n[:, own]
+    rk_ref[...] = k_r[:, own]
+
+
+def head_call(x_all, w_head, g_head, cosine, sine, q_gain, k_gain):
+    seq = x_all.shape[0]
+    width = HEAD_WIDTH
+    half = seq // 2
+    f32, bf16 = jnp.float32, jnp.bfloat16
+    tile = 256
+    return pl.pallas_call(
+        functools.partial(head_kernel, tile),
+        out_shape=(
+            jax.ShapeDtypeStruct((width, seq), bf16),
+            jax.ShapeDtypeStruct((2, width, half), f32),
+            jax.ShapeDtypeStruct((2, width, half), bf16),
+            jax.ShapeDtypeStruct((width, half), f32),
+            jax.ShapeDtypeStruct((1, half), f32),
+        ),
+        in_specs=[pl.BlockSpec(memory_space=pltpu.VMEM)] * 7,
+        out_specs=[pl.BlockSpec(memory_space=pltpu.VMEM)] * 5,
+        scratch_shapes=[
+            pltpu.VMEM((width, seq), bf16),
+            pltpu.VMEM((width, seq), f32),
+            pltpu.VMEM((1, seq), f32),
+            pltpu.VMEM((width, seq), bf16),
+            pltpu.VMEM((width, seq), bf16),
+            pltpu.VMEM((seq, width), bf16),
+            pltpu.VMEM((seq, width), bf16),
+            pltpu.VMEM((width, seq), bf16),
+            pltpu.VMEM((width, seq), f32),
+            pltpu.VMEM((1, seq), f32),
+            pltpu.VMEM((width, seq), f32),
+            pltpu.VMEM((width, seq), f32),
+        ],
+        compiler_params=pltpu.CompilerParams(vmem_limit_bytes=VMEM_LIMIT),
+        name="one_head",
+    )(x_all, w_head, g_head, cosine, sine, q_gain, k_gain)
+
+
+def spread_kernel(
+    n, gq_ref, mine_ref, theirs_ref, kn_ref, rk_ref, cos_ref, sin_ref, kg_ref,
+    gq_all, gkv_all, landed, gkv, qsend, qrecv, ksend, krecv, own,
+):
+    me = lax.axis_index("sp")
+    mate = other_of_pair(me)
+    half = mine_ref.shape[2]
+
+    def place(index):
+        columns = pl.ds(pl.multiple_of(lax.rem(index, 2) * half, 128), half)
+        return gkv_all.at[:, index // 2, :, columns]
+
+    barrier = pltpu.get_barrier_semaphore()
+    for off in range(1, n):
+        pl.semaphore_signal(
+            barrier, inc=1, device_id={"sp": lax.rem(me + off, n)}, device_id_type=MESH
+        )
+    pl.semaphore_wait(barrier, n - 1)
+    swap = pltpu.make_async_remote_copy(
+        src_ref=theirs_ref,
+        dst_ref=landed,
+        send_sem=own.at[0],
+        recv_sem=own.at[1],
+        device_id={"sp": mate},
+        device_id_type=MESH,
+    )
+    swap.start()
+
+    def copy_q(off):
+        return pltpu.make_async_remote_copy(
+            src_ref=gq_ref,
+            dst_ref=gq_all.at[me],
+            send_sem=qsend.at[off - 1],
+            recv_sem=qrecv.at[off - 1],
+            device_id={"sp": lax.rem(me + off, n)},
+            device_id_type=MESH,
+        )
+
+    def copy_k(off):
+        return pltpu.make_async_remote_copy(
+            src_ref=gkv,
+            dst_ref=place(me),
+            send_sem=ksend.at[off - 1],
+            recv_sem=krecv.at[off - 1],
+            device_id={"sp": lax.rem(me + off, n)},
+            device_id_type=MESH,
+        )
+
+    for off in range(1, n):
+        copy_q(off).start()
+    own_q = pltpu.make_async_copy(gq_ref, gq_all.at[me], own.at[2])
+    own_q.start()
+    swap.wait()
+    dkey = mine_ref[0] + landed[0].astype(jnp.float32)
+    back = dkey * cos_ref[...] + turn_back(dkey * sin_ref[...])
+    gkv[0] = norm_cols_back(back, kn_ref[...], rk_ref[...], kg_ref[...]).astype(jnp.bfloat16)
+    gkv[1] = (mine_ref[1] + landed[1].astype(jnp.float32)).astype(jnp.bfloat16)
+    for off in range(1, n):
+        copy_k(off).start()
+    own_k = pltpu.make_async_copy(gkv, place(me), own.at[3])
+    own_k.start()
+    for off in range(1, n):
+        source = lax.rem(me + n - off, n)
+        copy_q(off).wait_send()
+        copy_k(off).wait_send()
+        pltpu.make_async_remote_copy(
+            src_ref=gq_ref,
+            dst_ref=gq_all.at[source],
+            send_sem=qsend.at[off - 1],
+            recv_sem=qrecv.at[off - 1],
+            device_id={"sp": source},
+            device_id_type=MESH,
+        ).wait_recv()
+        pltpu.make_async_remote_copy(
+            src_ref=gkv,
+            dst_ref=place(source),
+            send_sem=ksend.at[off - 1],
+            recv_sem=krecv.at[off - 1],
+            device_id={"sp": source},
+            device_id_type=MESH,
+        ).wait_recv()
+    own_q.wait()
+    own_k.wait()
+
+
+def spread_call(n, gq, mine, theirs, k_normed, k_inv, cosine, sine, k_gain):
+    width, seq = gq.shape
+    half = seq // 2
+    bf16 = jnp.bfloat16
+    dma = pltpu.SemaphoreType.DMA
+    return pl.pallas_call(
+        functools.partial(spread_kernel, n),
+        out_shape=(
+            jax.ShapeDtypeStruct((n, width, seq), bf16),
+            jax.ShapeDtypeStruct((2, n // 2, width, seq), bf16),
+        ),
+        in_specs=[pl.BlockSpec(memory_space=pltpu.VMEM)] * 8,
+        out_specs=[pl.BlockSpec(memory_space=pl.ANY)] * 2,
+        scratch_shapes=[
+            pltpu.VMEM((2, width, half), bf16),
+            pltpu.VMEM((2, width, half), bf16),
+            dma((n - 1,)),
+            dma((n - 1,)),
+            dma((n - 1,)),
+            dma((n - 1,)),
+            dma((4,)),
+        ],
+        compiler_params=pltpu.CompilerParams(
+            collective_id=1, has_side_effects=True, vmem_limit_bytes=VMEM_LIMIT
+        ),
+        name="spread_grads",
+    )(gq, mine, theirs, k_normed, k_inv, cosine, sine, k_gain)
+
+
+def axial_columns(seq):
+    quarter = HEAD_WIDTH // 4
+    freqs = axial_base ** (-jnp.arange(quarter, dtype=jnp.float32) / quarter)
+    grid_rows = -(-seq // GRID_W)
+    by_row = freqs[:, None] * jnp.arange(grid_rows, dtype=jnp.float32)[None, :]
+    by_col = freqs[:, None] * jnp.arange(GRID_W, dtype=jnp.float32)[None, :]
+
+    def table(function):
+        rows = jnp.repeat(function(by_row), GRID_W, axis=1)[:, :seq]
+        cols = jnp.tile(function(by_col), (1, grid_rows))[:, :seq]
+        return jnp.concatenate([rows, rows, cols, cols], axis=0)
+
+    return table(jnp.cos), table(jnp.sin)
+
+
+def head_body(n, inputs, w_query, w_key, w_value, query_gain, key_gain, grad_out):
+    rows = inputs.shape[0]
+    seq = rows * n
+    width = HEAD_WIDTH
+    me = lax.axis_index("sp")
+    g_parts = grad_out.reshape(rows, n, width).transpose(1, 0, 2)
+    cosine, sine = axial_columns(seq)
+    w_head = jnp.concatenate(
+        [
+            lax.dynamic_slice_in_dim(w_query, me * width, width, 0),
+            lax.dynamic_slice_in_dim(w_key, (me // 2) * width, width, 0),
+            lax.dynamic_slice_in_dim(w_value, (me // 2) * width, width, 0),
+        ],
+        axis=0,
+    )
+    q_gain = query_gain[:, None]
+    k_gain = key_gain[:, None]
+    x_all, g_all = gather_call(n, inputs, g_parts)
+    x_all = x_all.reshape(seq, inputs.shape[1])
+    gq, mine, theirs, k_normed, k_inv = head_call(
+        x_all, w_head, g_all.reshape(seq, width), cosine, sine, q_gain, k_gain
+    )
+    half = seq // 2
+    start = (me % 2) * half
+    gq_all, gkv_all = spread_call(
+        n, gq, mine, theirs, k_normed, k_inv,
+        lax.dynamic_slice_in_dim(cosine, start, half, 1),
+        lax.dynamic_slice_in_dim(sine, start, half, 1),
+        k_gain,
+    )
+    grads = [
+        gq_all.reshape(n * width, seq),
+        gkv_all[0].reshape(n // 2 * width, seq),
+        gkv_all[1].reshape(n // 2 * width, seq),
+    ]
+    head_part = 0.0
+    for grad, weight in zip(grads, (w_query, w_key, w_value)):
+        own = lax.dynamic_slice_in_dim(grad, me * rows, rows, 1)
+        head_part = head_part + lax.dot_general(
+            own, weight, (((0,), (0,)), ((), ())), preferred_element_type=jnp.float32
+        )
+    d_inputs = lax.psum_scatter(
+        head_part.astype(jnp.bfloat16), "dp", scatter_dimension=1, tiled=True
+    )
+    outs = [jnp.dot(grad, x_all, preferred_element_type=jnp.float32) for grad in grads]
+    return (d_inputs, *outs)
+
+
 def solution(mesh):
+    n_sp = mesh.shape["sp"]
+    n_dp = mesh.shape["dp"]
+
+    def whole_body(inputs, w_query, w_key, *rest):
+        heads = w_query.shape[0] // HEAD_WIDTH
+        rows = inputs.shape[0]
+        fits = heads == n_sp and w_query.shape[0] == 2 * w_key.shape[0] and n_dp % 2 == 0
+        if fits and n_sp % 2 == 0 and rows % 32 == 0 and (rows * n_sp) % 256 == 0:
+            return head_body(n_sp, inputs, w_query, w_key, *rest)
+        return body(inputs, w_query, w_key, *rest)
+
     return jax.shard_map(
-        body,
+        whole_body,
         mesh=mesh,
         in_specs=(
             P("sp", None),

time: 500 us -> 242 us (0.48)
  waiting for transfers between devices: 373 us -> 18.7 us
  Pallas kernels: 0 us -> 169 us
  local copies, waits for them, and re-layouts: 54.1 us -> 15.5 us
  matrix products: 40.2 us -> 22.6 us
  other arithmetic: 16.9 us -> 1.18 us
    psum x1 -> x0, waiting for transfers between devices: 266 us -> none  [body(): grad_wq, grad_wkv = lax.psum((grad_wq, grad_wkv), 'sp')]
    pallas_call x0 -> x3, Pallas kernels: none -> 169 us  [the longest x1 84.3 us: spread_call(): pl.pallas_call(functools.partial(spread_kernel, n), out_shape=(jax.ShapeD...]
    reduce_scatter x2 -> x1, waiting for transfers between devices: 71.6 us -> 18.6 us  [head_body(): lax.psum_scatter(head_part.astype(jnp.bfloat16), 'dp', scatter_dimension=...]
    all_gather x1 -> x0, waiting for transfers between devices: 35.3 us -> none  [body(): kv_every = lax.all_gather(kv_rot, 'sp', axis=0, tiled=True)]
    unnamed x112 -> x31, local copies, waits for them, and re-layouts: 26.3 us -> 4.25 us
    dot_general x54 -> x6, matrix products: 40.2 us -> 22.6 us  [the longest x3 17 us: head_body(): jnp.dot(grad, x_all, preferred_element_type=jnp.float32)]
    mul x15 -> x0, local copies, waits for them, and re-layouts: 12.1 us -> none  [the longest x4 3.44 us: head_norm_back(): normed * jnp.mean(scaled * normed, axis=-1, keepdims=True)]
    slice x5 -> x1, local copies, waits for them, and re-layouts: 9.72 us -> 2.61 us  [head_body(): gkv_all[1].reshape(n // 2 * width, seq)]
  transfers between devices with their start and end apart: 4 -> 1, of which waited for: 4 -> 1; matrix products, arithmetic and copies ran while one was open for 8% -> 7% of each run, Pallas kernels for 0% -> 0%
where the time goes in v1:
time: 242 us
  Pallas kernels  169 us (70%)
  matrix products  22.6 us (9%)
  waiting for transfers between devices  18.7 us (8%)
  local copies, waits for them, and re-layouts  15.5 us (6%)
  between operations  14.3 us (6%)
    pallas_call x1, Pallas kernels, spread_call(): pl.pallas_call(functools.partial(spread_kernel, n), out_shape=(jax.ShapeD...  84.3 us
    pallas_call x1, Pallas kernels, gather_call(): pl.pallas_call(functools.partial(gather_kernel, n), out_shape=(jax.ShapeD...  64.5 us
    pallas_call x1, Pallas kernels, head_call(): pl.pallas_call(functools.partial(head_kernel, tile), out_shape=(jax.Shape...  20.6 us
    reduce_scatter x1, waiting for transfers between devices, head_body(): lax.psum_scatter(head_part.astype(jnp.bfloat16), 'dp', scatter_dimension=...  18.6 us
    dot_general x3, matrix products, head_body(): jnp.dot(grad, x_all, preferred_element_type=jnp.float32)  17 us
    dot_general x3, matrix products, head_body(): lax.dot_general(own, weight, (((0,), (0,)), ((), ())), preferred_element_...  5.61 us
  transfers between devices with their start and end apart: 1, of which 1 were waited for; matrix products, arithmetic and copies ran while one was open for 7% of the time, Pallas kernels for 0%

profile of v1, /device:TPU:0, one launch (start us, length us, event | category | flops | bytes accessed | tf_op | source)
XLA Modules:
  0.0 241.7 jit_solution(5282742750934297479)
XLA Ops:
  7.2 0.0 copy-start
  7.2 0.0 reduce-scatter.2.cloned.1.call-start
  7.2 0.1 fusion.7
  7.4 0.1 fusion.5
  7.5 1.2 copy.14
  8.8 0.9 copy.15
  9.7 0.0 copy-start.8
  9.7 0.0 copy-start.9
  9.7 0.1 broadcast_in_dim.20
  9.8 0.1 reshape.81
  10.0 0.1 tile.27
  10.1 0.0 copy-start.6
  10.1 0.1 broadcast_in_dim.21
  10.2 0.1 reshape.82
  10.3 0.7 constant_dynamic-update-slice_fusion.7
  10.9 0.6 constant_dynamic-update-slice_fusion.6
  11.6 0.7 tile.29
  12.3 0.0 copy-done.8
  12.3 0.7 copy.16.qg_ref
  13.1 0.0 copy-done.9
  13.1 0.7 copy.17.kg_ref
  13.8 0.0 copy-done.6
  13.8 0.0 copy-start.1
  13.8 1.6 constant_dynamic-update-slice_fusion.5
  15.4 1.6 constant_dynamic-update-slice_fusion
  17.0 0.0 copy-start.3
  17.0 0.7 constant_dynamic-slice_fusion.1.cos_ref
  17.8 1.6 constant_dynamic-slice_fusion.sin_ref
  19.4 64.5 %gather_tokens.1 = (bf16[8,192,2048]{2,1,0:T(8,128)(2,1)}, bf16[8,192,64]{2,1,0:T(8,128)(2,1)}) custom-call(bf16[192,2048]{1,0:T(8,128)(2,1)} %x_ref.1, bf16[8,192,64]{2,1,0:T(8,128)(2,1)} %bitcast.24), custom_call_target="tpu_custom_call" | custom-call | tf_op jit(solution)/shard_map/gather_tokens/pallas_call | solution.py:308
  83.9 0.0 copy-done
  83.9 0.0 copy-done.1
  84.0 1.0 constant_dynamic-slice_fusion.2
  84.9 0.0 copy-done.3
  85.0 0.9 pad_maximum_fusion.w_ref
  85.9 20.6 %one_head.1 = (bf16[64,1536]{1,0:T(8,128)(2,1)}, f32[2,64,768]{2,1,0:T(8,128)}, bf16[2,64,768]{2,1,0:T(8,128)(2,1)}, f32[64,768]{1,0:T(8,128)}, f32[1,768]{1,0:T(1,128)}) custom-call(bf16[1536,2048]{1,0:T(8,128)(2,1)} %bitcast.18, bf16[192,2048]{1,0:T(8,128)(2,1)} %pad_maximum_fusion.w_ref, bf16[1536,64]{1,0:T(8,128)(2,1)} %bitcast.30, ...), custom_call_target="tpu_custom_call" | custom-call | tf_op jit(solution)/shard_map/one_head/pallas_call | solution.py:403
  106.5 84.3 %spread_grads.1 = (bf16[8,64,1536]{2,1,0:T(8,128)(2,1)}, bf16[2,4,64,1536]{3,2,1,0:T(8,128)(2,1)}) custom-call(bf16[64,1536]{1,0:T(8,128)(2,1)} %get-tuple-element.15.gq_ref, f32[2,64,768]{2,1,0:T(8,128)} %get-tuple-element.16.mine_ref, bf16[2,64,768]{2,1,0:T(8,128)(2,1)} %get-tuple-element.17.theirs_ref, f32[64,768]{1,0:T(8,128)} %get-tuple-element.18.kn_ref, ...), custom_call_target="tpu_custom_call" | custom-call | tf_op jit(solution)/shard_map/spread_grads/pallas_call | solution.py:523
  190.8 2.6 %fusion.12 = (bf16[1,4,64,1536]{3,2,1,0:T(8,128)(2,1)}, bf16[1,4,64,1536]{3,2,1,0:T(8,128)(2,1)}) fusion(bf16[2,4,64,1536]{3,2,1,0:T(8,128)(2,1)} %get-tuple-element.21), kind=kLoop, calls=%fused_computation.31 | loop fusion | bytes 3145728 | tf_op jit(solution)/shard_map/slice | solution.py:595
  193.4 1.7 fusion.1
  195.1 0.0 copy-start.2
  195.1 1.5 convolution_add_fusion.1
  196.6 0.0 copy-done.2
  196.6 0.0 copy-start.4
  196.6 2.4 %fusion = bf16[192,2048]{1,0:T(8,128)(2,1)} fusion(f32[192,2048]{1,0:T(8,128)S(1)} %convolution_add_fusion.1, bf16[256,2048]{1,0:T(8,128)(2,1)S(1)} %copy-done.2, bf16[256,1536]{1,0:T(8,128)(2,1)} %bitcast.27, s32[]{:T(128)S(6)} %select_n.33), kind=kOutput, calls=%fused_computation.2 | convolution fusion | flops 202113024 | bytes 3538948 | tf_op jit(solution)/shard_map/dot_general | solution.py:600
  199.1 0.0 reduce-scatter.2.cloned.1.call-update
  199.1 0.0 copy-done.4
  199.1 0.0 copy-start.5
  199.1 0.0 slice-start
  199.1 6.0 %fusion.14 = f32[256,2048]{1,0:T(8,128)} fusion(bf16[256,1536]{1,0:T(8,128)(2,1)S(1)} %bitcast.26, bf16[1536,2048]{1,0:T(8,128)(2,1)} %bitcast.19), kind=kOutput, calls=%fused_computation.33 | convolution fusion | flops 1610612736 | bytes 9175040 | tf_op jit(solution)/shard_map/dot_general | solution.py:606
  205.2 0.0 copy-done.5
  205.2 0.0 slice-start.1
  205.2 0.0 copy-start.7
  205.2 6.0 %fusion.15 = f32[256,2048]{1,0:T(8,128)} fusion(bf16[256,1536]{1,0:T(8,128)(2,1)S(1)} %bitcast.28, bf16[1536,2048]{1,0:T(8,128)(2,1)} %bitcast.20), kind=kOutput, calls=%fused_computation.34 | convolution fusion | flops 1610612736 | bytes 9175040 | tf_op jit(solution)/shard_map/dot_general | solution.py:606
  211.2 0.0 slice-done
  211.2 0.0 slice-done.1
  211.2 0.0 copy-done.7
  211.2 4.9 %fusion.13 = f32[512,2048]{1,0:T(8,128)} fusion(bf16[512,1536]{1,0:T(8,128)(2,1)S(1)} %bitcast.32, bf16[1536,2048]{1,0:T(8,128)(2,1)S(1)} %bitcast.23), kind=kOutput, calls=%fused_computation.32 | convolution fusion | flops 3221225472 | bytes 12058624 | tf_op jit(solution)/shard_map/dot_general | solution.py:606
  216.2 18.6 %reduce-scatter.2.cloned.1.call-done = bf16[192,512]{1,0:T(8,128)(2,1)} async-done(((bf16[192,2048]{1,0:T(8,128)(2,1)}), bf16[192,512]{1,0:T(8,128)(2,1)}) %reduce-scatter.2.cloned.1.call-update) | async-done | bytes 196624 | tf_op jit(solution)/shard_map/reduce_scatter | solution.py:603
  (8 shorter events, 0.1 us)
Async XLA Ops:
  7.2 76.7 %copy-start = (bf16[512,2048]{1,0:T(8,128)(2,1)S(1)}, bf16[512,2048]{1,0:T(8,128)(2,1)}, u32[]{:S(2)}) copy-start(bf16[512,2048]{1,0:T(8,128)(2,1)} %param.8) | copy-start | bytes 6291460
  7.2 227.6 %reduce-scatter.2.cloned.1.call-start = ((), (), s32[]{:S(2)}) async-start(), calls=%async_computation.1 | async-start | bytes 983040 | tf_op jit(solution)/shard_map/reduce_scatter | solution.py:603
  9.7 2.7 %copy-start.8 = (f32[64]{0:T(128)S(1)}, f32[64]{0:T(128)}, u32[]{:S(2)}) copy-start(f32[64]{0:T(128)} %param.11) | copy-start | bytes 772
  9.7 3.4 %copy-start.9 = (f32[64]{0:T(128)S(1)}, f32[64]{0:T(128)}, u32[]{:S(2)}) copy-start(f32[64]{0:T(128)} %param.12) | copy-start | bytes 772
  10.1 3.7 %copy-start.6 = (f32[16,1536]{1,0:T(8,128)}, f32[16,1536]{1,0:T(8,128)S(1)}, u32[]{:S(2)}) copy-start(f32[16,1536]{1,0:T(8,128)S(1)} %tile.27) | copy-start | bytes 294916
  13.8 70.2 %copy-start.1 = (bf16[256,2048]{1,0:T(8,128)(2,1)S(1)}, bf16[256,2048]{1,0:T(8,128)(2,1)}, u32[]{:S(2)}) copy-start(bf16[256,2048]{1,0:T(8,128)(2,1)} %param.9) | copy-start | bytes 3145732
  17.0 67.9 %copy-start.3 = (f32[64,1536]{1,0:T(8,128)}, f32[64,1536]{1,0:T(8,128)S(1)}, u32[]{:S(2)}) copy-start(f32[64,1536]{1,0:T(8,128)S(1)} %get-tuple-element.30.cos_ref) | copy-start | bytes 1179652
  195.1 1.5 copy-start.2
  196.6 2.5 %copy-start.4 = (bf16[1,4,64,1536]{3,2,1,0:T(8,128)(2,1)S(1)}, bf16[1,4,64,1536]{3,2,1,0:T(8,128)(2,1)}, u32[]{:S(2)}) copy-start(bf16[1,4,64,1536]{3,2,1,0:T(8,128)(2,1)} %get-tuple-element.23) | copy-start | bytes 2359300
  199.1 6.1 %copy-start.5 = (bf16[1,4,64,1536]{3,2,1,0:T(8,128)(2,1)S(1)}, bf16[1,4,64,1536]{3,2,1,0:T(8,128)(2,1)}, u32[]{:S(2)}) copy-start(bf16[1,4,64,1536]{3,2,1,0:T(8,128)(2,1)} %get-tuple-element.22) | copy-start | bytes 2359300
  199.1 12.1 %slice-start = ((s8[6291456]{0:T(1024)(128)(4,1)}), s8[4194304]{0:T(1024)(128)(4,1)S(1)}, s32[]{:S(2)}) async-start(s8[6291456]{0:T(1024)(128)(4,1)} %bitcast.21), calls=%async_computation.2 | async-start | bytes 8388608
  205.2 6.1 %slice-start.1 = ((s8[6291456]{0:T(1024)(128)(4,1)}), s8[2097152]{0:T(1024)(128)(4,1)S(1)}, s32[]{:S(2)}) async-start(s8[6291456]{0:T(1024)(128)(4,1)} %bitcast.21), calls=%async_computation.3 | async-start | bytes 4194304
  205.2 6.1 %copy-start.7 = (bf16[8,64,1536]{2,1,0:T(8,128)(2,1)S(1)}, bf16[8,64,1536]{2,1,0:T(8,128)(2,1)}, u32[]{:S(2)}) copy-start(bf16[8,64,1536]{2,1,0:T(8,128)(2,1)} %get-tuple-element.20) | copy-start | bytes 4718596
Sparse Core Ops, SparseCore 0:
  199.2 35.5 reduce-scatter.1

commit v2 on v1

--- a/solution.py
+++ b/solution.py
@@ -243,40 +243,39 @@
                 device_id_type=MESH,
             )
         )
-        sends.append(
-            pltpu.make_async_remote_copy(
-                src_ref=x_ref.at[mine],
-                dst_ref=xall.at[me, mine],
-                send_sem=xsend.at[off - 1],
-                recv_sem=xrecv.at[off - 1],
-                device_id={"sp": peer},
-                device_id_type=MESH,
-            )
-        )
+    mate = other_of_pair(me)
+
+    def move(source, slot, device, part=mine, pair=(xsend, xrecv), first=False):
+        return pltpu.make_async_remote_copy(
+            src_ref=x_ref.at[mine] if first else xall.at[source, mine],
+            dst_ref=xall.at[source, part],
+            send_sem=pair[0].at[slot],
+            recv_sem=pair[1].at[slot],
+            device_id=device,
+            device_id_type=MESH,
+        )
+
+    for off in range(2, n, 2):
+        sends.append(move(me, off - 1, {"sp": lax.rem(me + off, n)}, first=True))
+    sends.append(move(me, 0, {"sp": mate}, first=True))
     for copy in sends:
         copy.start()
     own_x = pltpu.make_async_copy(x_ref, xall.at[me], own.at[0])
     own_g = pltpu.make_async_copy(g_ref.at[me], gall.at[me], own.at[1])
     own_x.start()
     own_g.start()
-    for off in range(1, n):
-        source = lax.rem(me + n - off, n)
-        pltpu.make_async_remote_copy(
-            src_ref=xall.at[source, mine],
-            dst_ref=xall.at[source, mine],
-            send_sem=xsend.at[off - 1],
-            recv_sem=xrecv.at[off - 1],
-            device_id={"sp": source},
-            device_id_type=MESH,
-        ).wait_recv()
-        pltpu.make_async_remote_copy(
-            src_ref=xall.at[source, mine],
-            dst_ref=xall.at[source, mine],
-            send_sem=fsend.at[off - 1],
-            recv_sem=frecv.at[off - 1],
-            device_id={"dp": twin},
-            device_id_type=MESH,
-        ).start()
+    forwards = (fsend, frecv)
+    for slot in range(0, n, 2):
+        source = lax.rem(mate + n - slot, n)
+        move(source, slot, {"sp": mate}).wait_recv()
+        move(source, slot, {"dp": twin}, pair=forwards).start()
+        if slot + 2 < n:
+            source = lax.rem(me + n - slot - 2, n)
+            move(source, slot + 1, {"sp": source}).wait_recv()
+            relay = move(source, slot + 2, {"sp": mate})
+            relay.start()
+            sends.append(relay)
+            move(source, slot + 1, {"dp": twin}, pair=forwards).start()
     for off in range(1, n):
         source = lax.rem(me + n - off, n)
         pltpu.make_async_remote_copy(
@@ -287,15 +286,10 @@
             device_id={"sp": source},
             device_id_type=MESH,
         ).wait_recv()
-        forward = pltpu.make_async_remote_copy(
-            src_ref=xall.at[source, mine],
-            dst_ref=xall.at[source, theirs],
-            send_sem=fsend.at[off - 1],
-            recv_sem=frecv.at[off - 1],
-            device_id={"dp": twin},
-            device_id_type=MESH,
-        )
-        forward.wait()
+    for slot in range(n - 1):
+        base = me if slot % 2 else mate
+        source = lax.rem(base + n - (slot + slot % 2), n)
+        move(source, slot, {"dp": twin}, part=theirs, pair=forwards).wait()
     for copy in sends:
         copy.wait_send()
     own_x.wait()
@@ -458,28 +452,34 @@
     )
     swap.start()
 
-    def copy_q(off):
+    def move_q(source, slot, device, first=False):
         return pltpu.make_async_remote_copy(
-            src_ref=gq_ref,
-            dst_ref=gq_all.at[me],
-            send_sem=qsend.at[off - 1],
-            recv_sem=qrecv.at[off - 1],
-            device_id={"sp": lax.rem(me + off, n)},
+            src_ref=gq_ref if first else gq_all.at[source],
+            dst_ref=gq_all.at[source],
+            send_sem=qsend.at[slot],
+            recv_sem=qrecv.at[slot],
+            device_id={"sp": device},
             device_id_type=MESH,
         )
 
-    def copy_k(off):
+    def move_k(source, slot, device, first=False):
         return pltpu.make_async_remote_copy(
-            src_ref=gkv,
-            dst_ref=place(me),
-            send_sem=ksend.at[off - 1],
-            recv_sem=krecv.at[off - 1],
-            device_id={"sp": lax.rem(me + off, n)},
+            src_ref=gkv if first else place(source),
+            dst_ref=place(source),
+            send_sem=ksend.at[slot],
+            recv_sem=krecv.at[slot],
+            device_id={"sp": device},
             device_id_type=MESH,
         )
 
-    for off in range(1, n):
-        copy_q(off).start()
+    def start_all(move):
+        copies = [move(me, off - 1, lax.rem(me + off, n), True) for off in range(2, n, 2)]
+        copies.append(move(me, 0, mate, True))
+        for copy in copies:
+            copy.start()
+        return copies
+
+    sends = start_all(move_q)
     own_q = pltpu.make_async_copy(gq_ref, gq_all.at[me], own.at[2])
     own_q.start()
     swap.wait()
@@ -487,30 +487,22 @@
     back = dkey * cos_ref[...] + turn_back(dkey * sin_ref[...])
     gkv[0] = norm_cols_back(back, kn_ref[...], rk_ref[...], kg_ref[...]).astype(jnp.bfloat16)
     gkv[1] = (mine_ref[1] + landed[1].astype(jnp.float32)).astype(jnp.bfloat16)
-    for off in range(1, n):
-        copy_k(off).start()
+    sends += start_all(move_k)
     own_k = pltpu.make_async_copy(gkv, place(me), own.at[3])
     own_k.start()
-    for off in range(1, n):
-        source = lax.rem(me + n - off, n)
-        copy_q(off).wait_send()
-        copy_k(off).wait_send()
-        pltpu.make_async_remote_copy(
-            src_ref=gq_ref,
-            dst_ref=gq_all.at[source],
-            send_sem=qsend.at[off - 1],
-            recv_sem=qrecv.at[off - 1],
-            device_id={"sp": source},
-            device_id_type=MESH,
-        ).wait_recv()
-        pltpu.make_async_remote_copy(
-            src_ref=gkv,
-            dst_ref=place(source),
-            send_sem=ksend.at[off - 1],
-            recv_sem=krecv.at[off - 1],
-            device_id={"sp": source},
-            device_id_type=MESH,
-        ).wait_recv()
+    for move in (move_q, move_k):
+        for slot in range(0, n, 2):
+            if slot + 2 < n:
+                source = lax.rem(me + n - slot - 2, n)
+                move(source, slot + 1, source).wait_recv()
+                relay = move(source, slot + 2, mate)
+                relay.start()
+                sends.append(relay)
+    for move in (move_q, move_k):
+        for slot in range(0, n, 2):
+            move(lax.rem(mate + n - slot, n), slot, mate).wait_recv()
+    for copy in sends:
+        copy.wait_send()
     own_q.wait()
     own_k.wait()
 

time: 242 us -> 201 us (0.83)
  Pallas kernels: 169 us -> 138 us
  waiting for transfers between devices: 18.7 us -> 8.84 us
    pallas_call x1, Pallas kernels: 84.3 us -> 52.7 us  [spread_call(): pl.pallas_call(functools.partial(spread_kernel, n), out_shape=(jax.ShapeD...]
    reduce_scatter x1, waiting for transfers between devices: 18.6 us -> 8.83 us  [head_body(): lax.psum_scatter(head_part.astype(jnp.bfloat16), 'dp', scatter_dimension=...]
  transfers between devices with their start and end apart: 1 -> 1, of which waited for: 1 -> 1; matrix products, arithmetic and copies ran while one was open for 7% -> 9% of each run, Pallas kernels for 0% -> 0%
where the time goes in v2:
time: 201 us
  Pallas kernels  138 us (69%)
  matrix products  22.8 us (11%)
  local copies, waits for them, and re-layouts  15.5 us (8%)
  between operations  14.3 us (7%)
  waiting for transfers between devices  8.84 us (4%)
    pallas_call x1, Pallas kernels, gather_call(): pl.pallas_call(functools.partial(gather_kernel, n), out_shape=(jax.ShapeD...  64.7 us
    pallas_call x1, Pallas kernels, spread_call(): pl.pallas_call(functools.partial(spread_kernel, n), out_shape=(jax.ShapeD...  52.7 us
    pallas_call x1, Pallas kernels, head_call(): pl.pallas_call(functools.partial(head_kernel, tile), out_shape=(jax.Shape...  20.6 us
    dot_general x3, matrix products, head_body(): jnp.dot(grad, x_all, preferred_element_type=jnp.float32)  17.2 us
    reduce_scatter x1, waiting for transfers between devices, head_body(): lax.psum_scatter(head_part.astype(jnp.bfloat16), 'dp', scatter_dimension=...  8.83 us
    dot_general x3, matrix products, head_body(): lax.dot_general(own, weight, (((0,), (0,)), ((), ())), preferred_element_...  5.61 us
    unnamed x31, local copies, waits for them, and re-layouts  4.25 us
  transfers between devices with their start and end apart: 1, of which 1 were waited for; matrix products, arithmetic and copies ran while one was open for 9% of the time, Pallas kernels for 0%

profile of v2, /device:TPU:0, one launch (start us, length us, event | category | flops | bytes accessed | tf_op | source)
XLA Modules:
  0.0 200.6 jit_solution(3249374801936542707)
XLA Ops:
  7.2 0.0 copy-start
  7.2 0.0 reduce-scatter.2.cloned.1.call-start
  7.2 0.1 fusion.7
  7.4 0.1 fusion.5
  7.5 1.2 copy.14
  8.8 0.9 copy.15
  9.7 0.0 copy-start.8
  9.7 0.0 copy-start.9
  9.7 0.1 broadcast_in_dim.20
  9.8 0.1 reshape.81
  10.0 0.1 tile.27
  10.1 0.0 copy-start.6
  10.1 0.1 broadcast_in_dim.21
  10.2 0.1 reshape.82
  10.3 0.7 constant_dynamic-update-slice_fusion.7
  10.9 0.6 constant_dynamic-update-slice_fusion.6
  11.6 0.7 tile.29
  12.3 0.0 copy-done.8
  12.3 0.7 copy.16.qg_ref
  13.1 0.0 copy-done.9
  13.1 0.7 copy.17.kg_ref
  13.8 0.0 copy-done.6
  13.8 0.0 copy-start.1
  13.8 1.6 constant_dynamic-update-slice_fusion.5
  15.4 1.6 constant_dynamic-update-slice_fusion
  17.0 0.0 copy-start.3
  17.0 0.7 constant_dynamic-slice_fusion.1.cos_ref
  17.8 1.6 constant_dynamic-slice_fusion.sin_ref
  19.4 64.7 %gather_tokens.1 = (bf16[8,192,2048]{2,1,0:T(8,128)(2,1)}, bf16[8,192,64]{2,1,0:T(8,128)(2,1)}) custom-call(bf16[192,2048]{1,0:T(8,128)(2,1)} %x_ref.1, bf16[8,192,64]{2,1,0:T(8,128)(2,1)} %bitcast.24), custom_call_target="tpu_custom_call" | custom-call | tf_op jit(solution)/shard_map/gather_tokens/pallas_call | solution.py:302
  84.1 0.0 copy-done
  84.1 0.0 copy-done.1
  84.1 1.0 constant_dynamic-slice_fusion.2
  85.1 0.0 copy-done.3
  85.2 0.9 pad_maximum_fusion.w_ref
  86.1 20.6 %one_head.1 = (bf16[64,1536]{1,0:T(8,128)(2,1)}, f32[2,64,768]{2,1,0:T(8,128)}, bf16[2,64,768]{2,1,0:T(8,128)(2,1)}, f32[64,768]{1,0:T(8,128)}, f32[1,768]{1,0:T(1,128)}) custom-call(bf16[1536,2048]{1,0:T(8,128)(2,1)} %bitcast.18, bf16[192,2048]{1,0:T(8,128)(2,1)} %pad_maximum_fusion.w_ref, bf16[1536,64]{1,0:T(8,128)(2,1)} %bitcast.30, ...), custom_call_target="tpu_custom_call" | custom-call | tf_op jit(solution)/shard_map/one_head/pallas_call | solution.py:397
  106.7 52.7 %spread_grads.1 = (bf16[8,64,1536]{2,1,0:T(8,128)(2,1)}, bf16[2,4,64,1536]{3,2,1,0:T(8,128)(2,1)}) custom-call(bf16[64,1536]{1,0:T(8,128)(2,1)} %get-tuple-element.15.gq_ref, f32[2,64,768]{2,1,0:T(8,128)} %get-tuple-element.16.mine_ref, bf16[2,64,768]{2,1,0:T(8,128)(2,1)} %get-tuple-element.17.theirs_ref, f32[64,768]{1,0:T(8,128)} %get-tuple-element.18.kn_ref, ...), custom_call_target="tpu_custom_call" | custom-call | tf_op jit(solution)/shard_map/spread_grads/pallas_call | solution.py:515
  159.4 2.6 %fusion.12 = (bf16[1,4,64,1536]{3,2,1,0:T(8,128)(2,1)}, bf16[1,4,64,1536]{3,2,1,0:T(8,128)(2,1)}) fusion(bf16[2,4,64,1536]{3,2,1,0:T(8,128)(2,1)} %get-tuple-element.21), kind=kLoop, calls=%fused_computation.31 | loop fusion | bytes 3145728 | tf_op jit(solution)/shard_map/slice | solution.py:587
  162.0 1.7 fusion.1
  163.7 0.0 copy-start.2
  163.7 1.5 convolution_add_fusion.1
  165.2 0.0 copy-done.2
  165.2 0.0 copy-start.4
  165.2 2.4 %fusion = bf16[192,2048]{1,0:T(8,128)(2,1)} fusion(f32[192,2048]{1,0:T(8,128)S(1)} %convolution_add_fusion.1, bf16[256,2048]{1,0:T(8,128)(2,1)S(1)} %copy-done.2, bf16[256,1536]{1,0:T(8,128)(2,1)} %bitcast.27, s32[]{:T(128)S(6)} %select_n.33), kind=kOutput, calls=%fused_computation.2 | convolution fusion | flops 202113024 | bytes 3538948 | tf_op jit(solution)/shard_map/dot_general | solution.py:592
  167.7 0.0 reduce-scatter.2.cloned.1.call-update
  167.7 0.0 copy-done.4
  167.7 0.0 copy-start.5
  167.7 0.0 slice-start
  167.7 6.0 %fusion.14 = f32[256,2048]{1,0:T(8,128)} fusion(bf16[256,1536]{1,0:T(8,128)(2,1)S(1)} %bitcast.26, bf16[1536,2048]{1,0:T(8,128)(2,1)} %bitcast.19), kind=kOutput, calls=%fused_computation.33 | convolution fusion | flops 1610612736 | bytes 9175040 | tf_op jit(solution)/shard_map/dot_general | solution.py:598
  173.8 0.0 copy-done.5
  173.8 0.0 slice-start.1
  173.8 0.0 copy-start.7
  173.8 6.2 %fusion.15 = f32[256,2048]{1,0:T(8,128)} fusion(bf16[256,1536]{1,0:T(8,128)(2,1)S(1)} %bitcast.28, bf16[1536,2048]{1,0:T(8,128)(2,1)} %bitcast.20), kind=kOutput, calls=%fused_computation.34 | convolution fusion | flops 1610612736 | bytes 9175040 | tf_op jit(solution)/shard_map/dot_general | solution.py:598
  180.0 0.0 slice-done
  180.0 0.0 slice-done.1
  180.0 0.0 copy-done.7
  180.0 4.9 %fusion.13 = f32[512,2048]{1,0:T(8,128)} fusion(bf16[512,1536]{1,0:T(8,128)(2,1)S(1)} %bitcast.32, bf16[1536,2048]{1,0:T(8,128)(2,1)S(1)} %bitcast.23), kind=kOutput, calls=%fused_computation.32 | convolution fusion | flops 3221225472 | bytes 12058624 | tf_op jit(solution)/shard_map/dot_general | solution.py:598
  184.9 8.8 %reduce-scatter.2.cloned.1.call-done = bf16[192,512]{1,0:T(8,128)(2,1)} async-done(((bf16[192,2048]{1,0:T(8,128)(2,1)}), bf16[192,512]{1,0:T(8,128)(2,1)}) %reduce-scatter.2.cloned.1.call-update) | async-done | bytes 196624 | tf_op jit(solution)/shard_map/reduce_scatter | solution.py:595
  (8 shorter events, 0.1 us)
Async XLA Ops:
  7.2 76.9 %copy-start = (bf16[512,2048]{1,0:T(8,128)(2,1)S(1)}, bf16[512,2048]{1,0:T(8,128)(2,1)}, u32[]{:S(2)}) copy-start(bf16[512,2048]{1,0:T(8,128)(2,1)} %param.8) | copy-start | bytes 6291460
  7.2 186.6 %reduce-scatter.2.cloned.1.call-start = ((), (), s32[]{:S(2)}) async-start(), calls=%async_computation.1 | async-start | bytes 983040 | tf_op jit(solution)/shard_map/reduce_scatter | solution.py:595
  9.7 2.7 %copy-start.8 = (f32[64]{0:T(128)S(1)}, f32[64]{0:T(128)}, u32[]{:S(2)}) copy-start(f32[64]{0:T(128)} %param.11) | copy-start | bytes 772
  9.7 3.4 %copy-start.9 = (f32[64]{0:T(128)S(1)}, f32[64]{0:T(128)}, u32[]{:S(2)}) copy-start(f32[64]{0:T(128)} %param.12) | copy-start | bytes 772
  10.1 3.7 %copy-start.6 = (f32[16,1536]{1,0:T(8,128)}, f32[16,1536]{1,0:T(8,128)S(1)}, u32[]{:S(2)}) copy-start(f32[16,1536]{1,0:T(8,128)S(1)} %tile.27) | copy-start | bytes 294916
  13.8 70.4 %copy-start.1 = (bf16[256,2048]{1,0:T(8,128)(2,1)S(1)}, bf16[256,2048]{1,0:T(8,128)(2,1)}, u32[]{:S(2)}) copy-start(bf16[256,2048]{1,0:T(8,128)(2,1)} %param.9) | copy-start | bytes 3145732
  17.0 68.1 %copy-start.3 = (f32[64,1536]{1,0:T(8,128)}, f32[64,1536]{1,0:T(8,128)S(1)}, u32[]{:S(2)}) copy-start(f32[64,1536]{1,0:T(8,128)S(1)} %get-tuple-element.30.cos_ref) | copy-start | bytes 1179652
  163.7 1.5 copy-start.2
  165.2 2.5 %copy-start.4 = (bf16[1,4,64,1536]{3,2,1,0:T(8,128)(2,1)S(1)}, bf16[1,4,64,1536]{3,2,1,0:T(8,128)(2,1)}, u32[]{:S(2)}) copy-start(bf16[1,4,64,1536]{3,2,1,0:T(8,128)(2,1)} %get-tuple-element.23) | copy-start | bytes 2359300
  167.7 6.1 %copy-start.5 = (bf16[1,4,64,1536]{3,2,1,0:T(8,128)(2,1)S(1)}, bf16[1,4,64,1536]{3,2,1,0:T(8,128)(2,1)}, u32[]{:S(2)}) copy-start(bf16[1,4,64,1536]{3,2,1,0:T(8,128)(2,1)} %get-tuple-element.22) | copy-start | bytes 2359300
  167.7 12.2 %slice-start = ((s8[6291456]{0:T(1024)(128)(4,1)}), s8[4194304]{0:T(1024)(128)(4,1)S(1)}, s32[]{:S(2)}) async-start(s8[6291456]{0:T(1024)(128)(4,1)} %bitcast.21), calls=%async_computation.2 | async-start | bytes 8388608
  173.8 6.2 %slice-start.1 = ((s8[6291456]{0:T(1024)(128)(4,1)}), s8[2097152]{0:T(1024)(128)(4,1)S(1)}, s32[]{:S(2)}) async-start(s8[6291456]{0:T(1024)(128)(4,1)} %bitcast.21), calls=%async_computation.3 | async-start | bytes 4194304
  173.8 6.2 %copy-start.7 = (bf16[8,64,1536]{2,1,0:T(8,128)(2,1)S(1)}, bf16[8,64,1536]{2,1,0:T(8,128)(2,1)}, u32[]{:S(2)}) copy-start(bf16[8,64,1536]{2,1,0:T(8,128)(2,1)} %get-tuple-element.20) | copy-start | bytes 4718596
Sparse Core Ops, SparseCore 0:
  167.8 25.8 reduce-scatter.1
